TPU v7x, 32 devices: a whole 2x2x4 slice. The times are simulated.
32 devices in a mesh: sp: 8 (over z, y), tp: 4 (over x, core).
Axes of the slice: x: 2, y: 2, z: 4, core: 2. Of those that a mesh axis runs over, the one named last changes fastest.
Arguments:
- activations: bfloat16 [4096, 2048], P('sp', 'tp'), may hold values from -250 to 250
- norm_gain: bfloat16 [2048], P('tp'), may hold values from 0.099609375 to 1.8984375
- pool_weight: bfloat16 [2048, 1024], P('sp', 'tp'), may hold values from -0.125 to 0.125
- gate_weight: bfloat16 [2048, 1024], P('sp', 'tp'), may hold values from -0.125 to 0.125
- value_weight: bfloat16 [2048, 1024], P('sp', 'tp'), may hold values from -0.125 to 0.125
- key_weight: bfloat16 [2048, 256], P('sp', 'tp'), may hold values from -0.125 to 0.125
- read_weight: bfloat16 [2048, 256], P('sp', 'tp'), may hold values from -0.125 to 0.125
- step_weight: bfloat16 [2048, 16], P('sp', 'tp'), may hold values from -0.125 to 0.125
- pool_mix: bfloat16 [4, 256, 256], P('tp'), may hold values from -0.375 to 0.375
- pool_scale: float32 [1024], P('tp'), may hold values from 0.1 to 1.9
- taps_value: float32 [4, 1024], P(None, 'tp'), may hold values from -3 to 3
- taps_key: float32 [4, 256], P(None, 'tp'), may hold values from -3 to 3
- taps_read: float32 [4, 256], P(None, 'tp'), may hold values from -3 to 3
- step_bias: float32 [16], P('tp'), may hold values from -1 to 1
- decay_log: float32 [16], P('tp')
- decay_extra: float32 [4096, 16], P('sp', 'tp'), may hold values from -1 to 0
- skip_scale: float32 [16], P('tp'), may hold values from 0.5 to 2
- state_gain: float32 [1024], P('tp'), may hold values from 0.1 to 1.9
- out_pool_weight: bfloat16 [1024, 2048], P('tp', 'sp'), may hold values from -0.125 to 0.125
- out_state_weight: bfloat16 [1024, 2048], P('tp', 'sp'), may hold values from -0.125 to 0.125
Outputs:
- mixed: bfloat16 [4096, 2048], P('sp', 'tp')
All inputs are finite; a program needn't handle non-finite values.
Results may differ from a plain program's by a relative error of at most 0.007.
Values may be sent and summed in bfloat16 or wider, within the bound.
A program may use at most 64 MiB of HBM per device.

v0:
```python
import jax
import jax.numpy as jnp
from jax import lax
from jax.sharding import PartitionSpec as P

SSM_STATE = 64
POOL_GROUPS = 4
SCAN_BLOCK = 128
MIX_W = 1024
EPSILON = 1e-06
HIGH = lax.Precision.HIGHEST


def shifted(value, axis, steps):
    count = lax.axis_size(axis)
    leading, last = (max(0, -steps), min(count, count - steps))
    return lax.ppermute(value, axis, [(source, source + steps) for source in range(leading, last)])


def carried_in(part, axis, combine, identity):
    place = lax.axis_index(axis)
    gathered = jax.tree.map(lambda a: lax.all_gather(a, axis), part)
    state = jax.tree.map(lambda a, e: jnp.zeros_like(a) + jnp.asarray(e, a.dtype), part, identity)

    def one(step, state):
        return combine(
            state, jax.tree.map(lambda a: lax.dynamic_index_in_dim(a, step, 0, False), gathered)
        )

    return lax.fori_loop(0, place, one, state)


def backward_kernel(extended, taps):
    width = taps.shape[0]
    length = extended.shape[0] - (width - 1)
    widened_rows = extended.astype(jnp.float32)
    total = jnp.zeros((length, extended.shape[1]), jnp.float32)
    for offset in range(width):
        total = total + taps[offset][None, :] * widened_rows[offset : offset + length]
    return jax.nn.silu(total).astype(jnp.bfloat16)


def combine_states(preceding_token, later):
    return (preceding_token[0] * later[0], preceding_token[1] * later[0][:, None, None] + later[1])


def local(
    activations,
    norm_gain,
    pool_weight,
    gate_weight,
    value_weight,
    key_weight,
    read_weight,
    step_weight,
    pool_mix,
    pool_scale,
    taps_value,
    taps_key,
    taps_read,
    step_bias,
    decay_log,
    decay_extra,
    skip_scale,
    state_gain,
    out_pool_weight,
    out_state_weight,
):
    length = activations.shape[0]
    cluster_span = pool_weight.shape[1]
    local_mix = gate_weight.shape[1]
    local_state = key_weight.shape[1]
    local_heads = step_weight.shape[1]
    joined = jnp.concatenate(
        [pool_weight, gate_weight, value_weight, key_weight, read_weight, step_weight], axis=1
    )
    in_weight = lax.all_gather(joined, "sp", axis=0, tiled=True)
    whole, gains = (
        lax.all_gather(activations, "tp", axis=1, tiled=True),
        lax.all_gather(norm_gain, "tp", axis=0, tiled=True),
    )
    widened_rows = whole.astype(jnp.float32)
    normed = (
        widened_rows
        * lax.rsqrt(jnp.mean(widened_rows * widened_rows, axis=-1, keepdims=True) + EPSILON)
        * gains.astype(jnp.float32)
    ).astype(jnp.bfloat16)
    projected = jnp.dot(normed, in_weight, preferred_element_type=jnp.float32)
    column = 0
    pool_in = projected[:, column : column + cluster_span].astype(jnp.bfloat16)
    column = column + cluster_span
    gate_in = projected[:, column : column + local_mix].astype(jnp.bfloat16)
    column = column + local_mix
    raw_value = projected[:, column : column + local_mix].astype(jnp.bfloat16)
    column = column + local_mix
    raw_key = projected[:, column : column + local_state].astype(jnp.bfloat16)
    column = column + local_state
    raw_read = projected[:, column : column + local_state].astype(jnp.bfloat16)
    column = column + local_state
    step_raw = projected[:, column : column + local_heads]
    raw_joined = jnp.concatenate([raw_value, raw_key, raw_read], axis=1)
    reach = 2**POOL_GROUPS - 1
    width = taps_value.shape[0]
    prior_pool, prior_joined = shifted(
        (pool_in[length - reach :], raw_joined[length - width + 1 :]), "sp", 1
    )
    group = lax.axis_index("tp")
    running = jnp.concatenate([prior_pool, pool_in], axis=0).astype(jnp.float32)
    levels = []
    for level in range(POOL_GROUPS):
        stride = 2**level
        running = running[stride:] + running[:-stride]
        levels.append(running[running.shape[0] - length :])
    window_sum = lax.dynamic_index_in_dim(jnp.stack(levels), group, 0, keepdims=False)
    window = jnp.exp2((group + 1).astype(jnp.float32))
    position = (lax.axis_index("sp") * length + jnp.arange(length, dtype=jnp.int32)).astype(
        jnp.float32
    )
    counts = jnp.minimum(position + 1.0, window)
    pooled = (window_sum / counts[:, None] - pool_in.astype(jnp.float32)).astype(jnp.bfloat16)
    pool_out = (
        jnp.dot(pooled, pool_mix[0], preferred_element_type=jnp.float32) * pool_scale
    ).astype(jnp.bfloat16)
    all_taps = jnp.concatenate([taps_value, taps_key, taps_read], axis=1)
    convolved = backward_kernel(jnp.concatenate([prior_joined, raw_joined], axis=0), all_taps)
    head_value = convolved[:, :local_mix]
    key_vectors = convolved[:, local_mix : local_mix + local_state]
    read_vectors = convolved[:, local_mix + local_state :]
    head_dim = local_mix // local_heads
    groups_here = local_state // SSM_STATE
    repeat = local_heads // groups_here
    blocks = length // SCAN_BLOCK
    step_size = jax.nn.softplus(step_raw + step_bias)
    log_decay = -jnp.exp(decay_log) * step_size + decay_extra
    value_heads = head_value.astype(jnp.float32).reshape(length, local_heads, head_dim)
    value_blocks = value_heads.reshape(blocks, SCAN_BLOCK, local_heads, head_dim)
    key_blocks = jnp.repeat(
        key_vectors.astype(jnp.float32).reshape(length, groups_here, SSM_STATE), repeat, axis=1
    ).reshape(blocks, SCAN_BLOCK, local_heads, SSM_STATE)
    read_blocks = jnp.repeat(
        read_vectors.astype(jnp.float32).reshape(length, groups_here, SSM_STATE), repeat, axis=1
    ).reshape(blocks, SCAN_BLOCK, local_heads, SSM_STATE)
    step_blocks = step_size.reshape(blocks, SCAN_BLOCK, local_heads)
    running_decay = jnp.cumsum(log_decay.reshape(blocks, SCAN_BLOCK, local_heads), axis=1)
    lower = jnp.arange(SCAN_BLOCK)[:, None] >= jnp.arange(SCAN_BLOCK)[None, :]
    gaps = jnp.where(
        lower[None, :, :, None],
        running_decay[:, :, None, :] - running_decay[:, None, :, :],
        -jnp.inf,
    )
    weights = jnp.einsum("blhn,bshn->blsh", read_blocks, key_blocks, precision=HIGH) * jnp.exp(gaps)
    scaled_value = value_blocks * step_blocks[..., None]
    inner = jnp.einsum("blsh,bshp->blhp", weights, scaled_value, precision=HIGH)
    block_ends = running_decay[:, -1, :]
    trailing = jnp.exp(block_ends[:, None, :] - running_decay)
    fresh = jnp.einsum("bshn,bsh,bshp->bhpn", key_blocks, trailing, scaled_value, precision=HIGH)

    def advance(carry, inputs):
        block_decay, block_state = inputs
        return (carry * block_decay[:, None, None] + block_state, carry)

    local_total, prefix = lax.scan(
        advance,
        jnp.zeros((local_heads, head_dim, SSM_STATE), jnp.float32),
        (jnp.exp(block_ends), fresh),
    )
    offsets = jnp.cumsum(block_ends, axis=0) - block_ends
    device_decay = jnp.exp(offsets[-1] + block_ends[-1])
    incoming_decay, incoming = carried_in(
        (device_decay, local_total),
        "sp",
        combine_states,
        (jnp.ones_like(device_decay), jnp.zeros_like(local_total)),
    )
    from_device = running_decay + offsets[:, None, :]
    local_off = (
        jnp.einsum("blhn,bhpn->blhp", read_blocks, prefix, precision=HIGH)
        * jnp.exp(running_decay)[..., None]
    )
    far_off = (
        jnp.einsum("blhn,hpn->blhp", read_blocks, incoming, precision=HIGH)
        * jnp.exp(from_device)[..., None]
    )
    scan_out = (inner + local_off + far_off).reshape(length, local_heads, head_dim) + skip_scale[
        None, :, None
    ] * value_heads
    gated = scan_out.reshape(length, local_mix) * jax.nn.silu(gate_in.astype(jnp.float32))
    gate_squares = lax.psum(jnp.sum(gated * gated, axis=-1), "tp")
    state_out = (gated * lax.rsqrt(gate_squares / MIX_W + EPSILON)[:, None] * state_gain).astype(
        jnp.bfloat16
    )
    branch_rows = jnp.concatenate([pool_out, state_out], axis=1)
    out_weight = jnp.concatenate([out_pool_weight, out_state_weight], axis=0)
    terms = jnp.dot(
        branch_rows,
        lax.all_gather(out_weight, "sp", axis=1, tiled=True),
        preferred_element_type=jnp.float32,
    )
    result = lax.psum_scatter(terms, "tp", scatter_dimension=1, tiled=True)
    return result.astype(jnp.bfloat16)


def solution(mesh):
    placed = (
        P("sp", "tp"),
        P("tp"),
        P("sp", "tp"),
        P("sp", "tp"),
        P("sp", "tp"),
        P("sp", "tp"),
        P("sp", "tp"),
        P("sp", "tp"),
        P("tp", None, None),
        P("tp"),
        P(None, "tp"),
        P(None, "tp"),
        P(None, "tp"),
        P("tp"),
        P("tp"),
        P("sp", "tp"),
        P("tp"),
        P("tp"),
        P("tp", "sp"),
        P("tp", "sp"),
    )
    return jax.shard_map(
        local, mesh=mesh, in_specs=placed, out_specs=P("sp", "tp"), check_vma=False
    )
```

profile of v0, /device:TPU:0, one launch (start us, length us, event | category | flops | bytes accessed | tf_op | source)
XLA Modules:
  0.0 262.7 jit_solution(2948103364905407184)
XLA Ops:
  7.4 0.9 copy.40
  8.2 0.9 copy.41
  10.0 1.8 concatenate.21
  13.3 6.2 %all-gather.1 = bf16[4,1,512]{2,1,0:T(2,128)(2,1)S(1)} all-gather(bf16[1,1,512]{2,1,0:T(2,128)(2,1)S(1)} %reshape.74), channel_id=1, replica_groups=mesh['sp'=8,'tp'=4] {'tp'}, dimensions={0}, use_global_device_ids=true | all-gather | bytes 5120 | tf_op jit(solution)/shard_map/all_gather | solution.py:80
  21.0 13.2 %all-gather.7.cloned.1.call-done = bf16[512,2048]{1,0:T(8,128)(2,1)} async-done(((bf16[512,512]{1,0:T(8,128)(2,1)}), bf16[512,2048]{1,0:T(8,128)(2,1)}) %all-gather.7.cloned.1.call-update) | async-done | bytes 2097168 | tf_op jit(solution)/shard_map/all_gather | solution.py:79
  34.3 2.2 fusion.1
  36.5 72.7 %all-gather.9.cloned.1.call-done = bf16[2048,900]{1,0:T(8,128)(2,1)} async-done(((bf16[256,900]{1,0:T(8,128)(2,1)}), bf16[2048,900]{1,0:T(8,128)(2,1)}) %all-gather.9.cloned.1.call-update) | async-done | bytes 3686416 | tf_op jit(solution)/shard_map/all_gather | solution.py:77
  109.2 4.5 %fusion.57 = (bf16[512,900]{0,1:T(8,128)(2,1)S(1)}, f32[512,900]{0,1:T(8,128)S(1)}) fusion(bf16[2048,900]{1,0:T(8,128)(2,1)} %all-gather.9.cloned.1.call-done, bf16[512,2048]{1,0:T(8,128)(2,1)S(1)} %copy-done.1, f32[2048]{0:T(1024)S(1)} %bitcast.113, f32[512]{0:T(512)S(1)} %add_rsqrt_fusion.1), kind=kOutput, calls=%fused_computation.113 | convolution fusion | flops 1892091904 | bytes 8558592 | tf_op jit(solution)/shard_map/dot_general | solution.py:88
  113.9 2.5 collective-permute-start.1
  120.1 4.6 %collective-permute-start = (bf16[15,256]{0,1:T(8,128)(2,1)}, bf16[15,256]{0,1:T(8,128)(2,1)}, u32[]{:S(2)}, u32[]{:S(2)}) collective-permute-start(bf16[15,256]{0,1:T(8,128)(2,1)} %slice.139), channel_id=1, source_target_pairs={{0,4},{4,8},{8,12},{12,16},{16,20},{20,24},{24,28},{1,5},{5,9},{9,... | collective-permute-start | bytes 23048 | tf_op jit(solution)/shard_map/ppermute | solution.py:17
  124.7 16.9 %all-gather.2 = f32[8,1,4]{2,1,0:T(1,128)} all-gather(f32[1,1,4]{2,1,0:T(1,128)S(1)} %fusion.49), channel_id=1, replica_groups=mesh['sp'=8,'tp'=4] {'sp'}, dimensions={0}, use_global_device_ids=true | all-gather | bytes 144 | tf_op jit(solution)/shard_map/all_gather | solution.py:22
  141.8 0.9 multiply_convert_fusion
  143.7 0.9 fusion.32
  144.6 3.1 %while.26 = (s32[]{:T(128)}, f32[4,64,64]{2,1,0:T(8,128)S(1)}, f32[4,4,64,64]{3,2,1,0:T(8,128)}, f32[4,4]{1,0:T(4,128)S(1)}, f32[4,4,64,64]{3,2,1,0:T(8,128)S(1)}, /*index=5*/s32[]{:T(128)}, s32[]{:T(128)}) while((s32[]{:T(128)}, f32[4,64,64]{2,1,0:T(8,128)S(1)}, f32[4,4,64,64]{3,2,1,0:T(8,128)}, f32[4,4]{1,0:T(4,128)S(1)}, ...), condition=%wide.region_3.4_spmd.clone, body=%wide.region_2.3_spmd.clone.sunk | while | flops 65539 | bytes 393872 | solution.py:162
  147.8 34.8 %all-gather = f32[32,64,64]{2,1,0:T(8,128)S(1)} all-gather(f32[4,64,64]{2,1,0:T(8,128)S(1)} %get-tuple-element.78), channel_id=2, replica_groups=mesh['sp'=8,'tp'=4] {'sp'}, dimensions={0}, use_global_device_ids=true | all-gather | bytes 589824 | tf_op jit(solution)/shard_map/all_gather | solution.py:22
  182.8 1.3 fusion.12
  184.1 1.6 fusion.11
  185.7 2.9 %fusion.8 = f32[4,128,128,4]{2,1,3,0:T(8,128)S(1)} fusion(f32[4,128,4]{1,2,0:T(4,128)} %copy.48, pred[128,128]{1,0:T(8,128)(4,1)} %iota_compare_fusion, f32[4,128,64]{1,2,0:T(8,128)S(1)} %get-tuple-element.147, f32[4,128,64]{1,2,0:T(8,128)} %copy-done.2), kind=kOutput, calls=%fused_computation.19 | convolution fusion | flops 202113024 | bytes 1335296 | tf_op jit(solution)/shard_map/blhn,bshn->blsh/dot_general | solution.py:151
  188.7 2.2 fusion.10
  191.5 5.7 %psum.7 = f32[512]{0:T(512)S(1)} all-reduce(f32[512]{0:T(512)S(1)} %get-tuple-element.132), channel_id=1, replica_groups=mesh['sp'=8,'tp'=4] {'tp'}, use_global_device_ids=true, to_apply=%region_8.9 | all-reduce | flops 512 | bytes 4096 | tf_op jit(solution)/shard_map/psum | solution.py:188
  197.3 1.0 maximum_convert_fusion.1
  200.1 4.8 %fusion.28 = f32[512,2048]{1,0:T(8,128)} fusion(bf16[512,2048]{1,0:T(8,128)(2,1)} %all-gather.11.cloned.1.call-done, bf16[512,256]{0,1:T(8,128)(2,1)S(1)} %multiply_convert_fusion.1, bf16[512,256]{0,1:T(8,128)(2,1)S(1)} %fusion.13), kind=kOutput, calls=%fused_computation.57 | convolution fusion | flops 1074790400 | bytes 6815744 | tf_op jit(solution)/shard_map/dot_general | solution.py:194
  205.0 49.1 %reduce-scatter.2.cloned.1.call-done = f32[512,512]{1,0:T(8,128)} async-done(((f32[512,2048]{1,0:T(8,128)}), f32[512,512]{1,0:T(8,128)}) %reduce-scatter.2.cloned.1.call-update) | async-done | bytes 1048592 | tf_op jit(solution)/shard_map/reduce_scatter | solution.py:199
  254.1 2.1 convert_element_type.70
  (105 shorter events, 15.3 us)
Async XLA Ops:
  6.5 193.0 %copy-start = (bf16[1,256,256]{2,1,0:T(8,128)(2,1)S(1)}, bf16[1,256,256]{2,1,0:T(8,128)(2,1)}, u32[]{:S(2)}) copy-start(bf16[1,256,256]{2,1,0:T(8,128)(2,1)} %param.32) | copy-start | bytes 393220
  6.5 5.3 %copy-start.4 = (bf16[256,256]{1,0:T(8,128)(2,1)S(1)}, bf16[256,256]{1,0:T(8,128)(2,1)}, u32[]{:S(2)}) copy-start(bf16[256,256]{1,0:T(8,128)(2,1)} %param.42) | copy-start | bytes 393220
  6.5 5.3 %copy-start.3 = (bf16[256,256]{1,0:T(8,128)(2,1)S(1)}, bf16[256,256]{1,0:T(8,128)(2,1)}, u32[]{:S(2)}) copy-start(bf16[256,256]{1,0:T(8,128)(2,1)} %param.43) | copy-start | bytes 393220
  6.5 6.8 %copy-start.12 = (bf16[512]{0:T(512)(128)(2,1)S(1)}, bf16[512]{0:T(512)(128)(2,1)}, u32[]{:S(2)}) copy-start(bf16[512]{0:T(512)(128)(2,1)} %param.25) | copy-start | bytes 3076
  6.5 12.9 %copy-start.6 = (f32[4,256]{1,0:T(4,128)S(1)}, f32[4,256]{1,0:T(4,128)}, u32[]{:S(2)}) copy-start(f32[4,256]{1,0:T(4,128)} %param.34) | copy-start | bytes 12292
  6.5 12.9 %copy-start.9 = (f32[4,64]{1,0:T(4,128)S(1)}, f32[4,64]{1,0:T(4,128)}, u32[]{:S(2)}) copy-start(f32[4,64]{1,0:T(4,128)} %param.35) | copy-start | bytes 3076
  6.6 12.9 %copy-start.8 = (f32[4,64]{1,0:T(4,128)S(1)}, f32[4,64]{1,0:T(4,128)}, u32[]{:S(2)}) copy-start(f32[4,64]{1,0:T(4,128)} %param.36) | copy-start | bytes 3076
  6.6 13.1 %copy-start.16 = (f32[4]{0:T(128)S(1)}, f32[4]{0:T(128)}, u32[]{:S(2)}) copy-start(f32[4]{0:T(128)} %param.38) | copy-start | bytes 52
  6.6 13.1 %copy-start.14 = (f32[4]{0:T(128)S(1)}, f32[4]{0:T(128)}, u32[]{:S(2)}) copy-start(f32[4]{0:T(128)} %param.40) | copy-start | bytes 52
  6.6 27.7 %all-gather.7.cloned.1.call-start = ((), (), s32[]{:S(2)}) async-start(), calls=%async_computation.1 | async-start | bytes 2621440 | tf_op jit(solution)/shard_map/all_gather | solution.py:79
  7.3 101.9 %all-gather.9.cloned.1.call-start = ((), (), s32[]{:S(2)}) async-start(), calls=%async_computation.2 | async-start | bytes 4718592 | tf_op jit(solution)/shard_map/all_gather | solution.py:77
  11.8 188.3 %all-gather.11.cloned.1.call-start = ((), (), s32[]{:S(2)}) async-start(), calls=%async_computation.3 | async-start | bytes 2359296 | tf_op jit(solution)/shard_map/all_gather | solution.py:196
  12.6 241.4 %reduce-scatter.2.cloned.1.call-start = ((), (), s32[]{:S(2)}) async-start(), calls=%async_computation.4 | async-start | bytes 5242880 | tf_op jit(solution)/shard_map/reduce_scatter | solution.py:199
  34.3 75.0 %copy-start.1 = (bf16[512,2048]{1,0:T(8,128)(2,1)S(1)}, bf16[512,2048]{1,0:T(8,128)(2,1)}, u32[]{:S(2)}) copy-start(bf16[512,2048]{1,0:T(8,128)(2,1)} %all-gather.7.cloned.1.call-done) | copy-start | bytes 6291460
  109.2 7.1 %copy-start.5 = (f32[512,4]{0,1:T(4,128)S(1)}, f32[512,4]{0,1:T(4,128)}, u32[]{:S(2)}) copy-start(f32[512,4]{0,1:T(4,128)} %param.39) | copy-start | bytes 24580
  109.2 7.1 %copy-start.13 = (f32[4]{0:T(128)S(1)}, f32[4]{0:T(128)}, u32[]{:S(2)}) copy-start(f32[4]{0:T(128)} %param.37) | copy-start | bytes 52
  113.9 27.7 %collective-permute-start.1 = (bf16[3,384]{0,1:T(8,128)(2,1)S(1)}, bf16[3,384]{0,1:T(8,128)(2,1)S(1)}, u32[]{:S(2)}, u32[]{:S(2)}) collective-permute-start(bf16[3,384]{0,1:T(8,128)(2,1)S(1)} %slice.152), channel_id=1, source_target_pairs={{0,4},{4,8},{8,12},{12,16},{16,20},{20,24},{24,28},{1,5},{5,9},{9,... | collective-permute-start | bytes 6920 | tf_op jit(solution)/shard_map/ppermute | solution.py:17
  120.1 77.1 %collective-permute-start = (bf16[15,256]{0,1:T(8,128)(2,1)}, bf16[15,256]{0,1:T(8,128)(2,1)}, u32[]{:S(2)}, u32[]{:S(2)}) collective-permute-start(bf16[15,256]{0,1:T(8,128)(2,1)} %slice.139), channel_id=1, source_target_pairs={{0,4},{4,8},{8,12},{12,16},{16,20},{20,24},{24,28},{1,5},{5,9},{9,... | collective-permute-start | bytes 23048 | tf_op jit(solution)/shard_map/ppermute | solution.py:17
  143.0 0.7 copy-start.2
  188.6 2.5 copy-start.7
  190.8 6.3 %copy-start.11 = (f32[256]{0:T(256)S(1)}, f32[256]{0:T(256)}, u32[]{:S(2)}) copy-start(f32[256]{0:T(256)} %param.41) | copy-start | bytes 3076
  199.0 0.7 copy-start.10
  199.0 0.7 copy-start.15
Sparse Core Ops, SparseCore 0:
  9.0 25.2 all-gather.6
  36.4 72.7 all-gather.8
  111.3 60.4 all-gather.10
  205.1 48.9 reduce-scatter.1
where the time goes:
time: 263 us
  waiting for transfers between devices  136 us (52%)
  blocking collectives  63.5 us (24%)
  matrix products  18.7 us (7%)
  between operations  13.6 us (5%)
  other arithmetic  13.4 us (5%)
  local copies, waits for them, and re-layouts  10.1 us (4%)
  starting transfers between devices  7.23 us (3%)
    all_gather x1, waiting for transfers between devices, local(): in_weight = lax.all_gather(joined, 'sp', axis=0, tiled=True)  72.7 us
    all_gather x2, blocking collectives, carried_in(): gathered = jax.tree.map(lambda a: lax.all_gather(a, axis), part)  51.7 us
    reduce_scatter x1, waiting for transfers between devices, local(): result = lax.psum_scatter(terms, 'tp', scatter_dimension=1, tiled=True)  49.1 us
    all_gather x1, waiting for transfers between devices, local(): lax.all_gather(activations, 'tp', axis=1, tiled=True)  13.2 us
    ppermute x2, starting transfers between devices, shifted(): lax.ppermute(value, axis, [(source, source + steps) for source in range(l...  7.07 us
    all_gather x1, blocking collectives, local(): lax.all_gather(norm_gain, 'tp', axis=0, tiled=True)  6.15 us
    psum x1, blocking collectives, local(): gate_squares = lax.psum(jnp.sum(gated * gated, axis=-1), 'tp')  5.66 us
  transfers between devices with their start and end apart: 6, of which 3 were waited for; matrix products, arithmetic and copies ran while one was open for 13% of the time, Pallas kernels for 0%

commit v1 on v0

--- a/solution.py
+++ b/solution.py
@@ -76,7 +76,9 @@
     )
     in_weight = lax.all_gather(joined, "sp", axis=0, tiled=True)
     whole, gains = (
-        lax.all_gather(activations, "tp", axis=1, tiled=True),
+        jnp.concatenate(
+            lax.all_to_all(jnp.stack([activations] * lax.axis_size("tp")), "tp", 0, 0), axis=1
+        ),
         lax.all_gather(norm_gain, "tp", axis=0, tiled=True),
     )
     widened_rows = whole.astype(jnp.float32)

time: 263 us -> 240 us (0.913)
  waiting for transfers between devices: 136 us -> 86.4 us
  blocking collectives: 63.5 us -> 83.6 us
  starting transfers between devices: 7.23 us -> 11.5 us
    all_gather x1, waiting for transfers between devices: 72.7 us -> 37.6 us  [local(): in_weight = lax.all_gather(joined, 'sp', axis=0, tiled=True)]
    all_gather x1, blocking collectives: 6.15 us -> 25.8 us  [local(): lax.all_gather(norm_gain, 'tp', axis=0, tiled=True)]
    all_gather x1 -> x0, waiting for transfers between devices: 13.2 us -> none  [local(): lax.all_gather(activations, 'tp', axis=1, tiled=True)]
    all_to_all x0 -> x1, starting transfers between devices: none -> 4.38 us  [local(): lax.all_to_all(jnp.stack([activations] * lax.axis_size('tp')), 'tp', 0, 0)]
  transfers between devices with their start and end apart: 6 -> 6, of which waited for: 3 -> 2; matrix products, arithmetic and copies ran while one was open for 13% -> 13% of each run, Pallas kernels for 0% -> 0%
where the time goes in v1:
time: 240 us; the launch traced here: 239 us
  waiting for transfers between devices  86.4 us (36%)
  blocking collectives  83.6 us (35%)
  matrix products  18.1 us (8%)
  between operations  13.7 us (6%)
  other arithmetic  13.6 us (6%)
  local copies, waits for them, and re-layouts  11.9 us (5%)
  starting transfers between devices  11.5 us (5%)
    all_gather x2, blocking collectives, carried_in(): gathered = jax.tree.map(lambda a: lax.all_gather(a, axis), part)  52.2 us
    reduce_scatter x1, waiting for transfers between devices, local(): result = lax.psum_scatter(terms, 'tp', scatter_dimension=1, tiled=True)  48.6 us
    all_gather x1, waiting for transfers between devices, local(): in_weight = lax.all_gather(joined, 'sp', axis=0, tiled=True)  37.6 us
    all_gather x1, blocking collectives, local(): lax.all_gather(norm_gain, 'tp', axis=0, tiled=True)  25.8 us
    ppermute x2, starting transfers between devices, shifted(): lax.ppermute(value, axis, [(source, source + steps) for source in range(l...  7.08 us
    psum x1, blocking collectives, local(): gate_squares = lax.psum(jnp.sum(gated * gated, axis=-1), 'tp')  5.66 us
    dot_general x1, matrix products, local(): projected = jnp.dot(normed, in_weight, preferred_element_type=jnp.float32)  4.98 us
    dot_general x1, matrix products, local(): jnp.dot(branch_rows, lax.all_gather(out_weight, 'sp', axis=1, tiled=True)...  4.84 us
  transfers between devices with their start and end apart: 6, of which 2 were waited for; matrix products, arithmetic and copies ran while one was open for 13% of the time, Pallas kernels for 0%

profile of v1, /device:TPU:0, one launch (start us, length us, event | category | flops | bytes accessed | tf_op | source)
XLA Modules:
  0.0 239.0 jit_solution(13504134465375346958)
XLA Ops:
  6.5 0.9 copy.61
  9.2 1.8 concatenate.21
  11.2 1.5 stack.22
  12.8 4.4 %all-to-all-start = ((bf16[4,512,512]{1,2,0:T(8,128)(2,1)}), bf16[4,512,512]{1,2,0:T(8,128)(2,1)S(1)}, u32[]{:S(2)}, u32[]{:S(2)}) async-start(bf16[4,512,512]{1,2,0:T(8,128)(2,1)} %stack.22), calls=%async_computation | async-start | bytes 4194304 | tf_op jit(solution)/shard_map/all_to_all | solution.py:80
  18.1 25.8 %all-gather.1 = bf16[4,1,512]{2,1,0:T(2,128)(2,1)S(1)} all-gather(bf16[1,1,512]{2,1,0:T(2,128)(2,1)S(1)} %reshape.81), channel_id=1, replica_groups=mesh['sp'=8,'tp'=4] {'tp'}, dimensions={0}, use_global_device_ids=true | all-gather | bytes 5120 | tf_op jit(solution)/shard_map/all_gather | solution.py:82
  47.1 1.9 fusion.2
  49.0 37.6 %all-gather.6.cloned.1.call-done = bf16[2048,900]{1,0:T(8,128)(2,1)} async-done(((bf16[256,900]{1,0:T(8,128)(2,1)}), bf16[2048,900]{1,0:T(8,128)(2,1)}) %all-gather.6.cloned.1.call-update) | async-done | bytes 3686416 | tf_op jit(solution)/shard_map/all_gather | solution.py:77
  86.7 5.0 %fusion.52 = (bf16[512,900]{0,1:T(8,128)(2,1)S(1)}, f32[512,900]{0,1:T(8,128)S(1)}) fusion(bf16[512,2048]{0,1:T(8,128)(2,1)} %fusion.2, bf16[2048,900]{1,0:T(8,128)(2,1)} %all-gather.6.cloned.1.call-done), kind=kOutput, calls=%fused_computation.109 | convolution fusion | flops 1887897600 | bytes 8548352 | tf_op jit(solution)/shard_map/dot_general | solution.py:90
  91.8 2.5 %collective-permute-start.1 = (bf16[3,384]{0,1:T(8,128)(2,1)S(1)}, bf16[3,384]{0,1:T(8,128)(2,1)S(1)}, u32[]{:S(2)}, u32[]{:S(2)}) collective-permute-start(bf16[3,384]{0,1:T(8,128)(2,1)S(1)} %slice.152), channel_id=1, source_target_pairs={{0,4},{4,8},{8,12},{12,16},{16,20},{20,24},{24,28},{1,5},{5,9},{9,... | collective-permute-start | bytes 6920 | tf_op jit(solution)/shard_map/ppermute | solution.py:17
  98.0 4.6 %collective-permute-start = (bf16[15,256]{0,1:T(8,128)(2,1)}, bf16[15,256]{0,1:T(8,128)(2,1)}, u32[]{:S(2)}, u32[]{:S(2)}) collective-permute-start(bf16[15,256]{0,1:T(8,128)(2,1)} %slice.139), channel_id=1, source_target_pairs={{0,4},{4,8},{8,12},{12,16},{16,20},{20,24},{24,28},{1,5},{5,9},{9,... | collective-permute-start | bytes 23048 | tf_op jit(solution)/shard_map/ppermute | solution.py:17
  102.6 17.2 %all-gather.2 = f32[8,1,4]{2,1,0:T(1,128)} all-gather(f32[1,1,4]{2,1,0:T(1,128)S(1)} %fusion.44), channel_id=1, replica_groups=mesh['sp'=8,'tp'=4] {'sp'}, dimensions={0}, use_global_device_ids=true | all-gather | bytes 144 | tf_op jit(solution)/shard_map/all_gather | solution.py:22
  120.1 0.9 multiply_convert_fusion
  121.4 0.9 fusion.27
  122.3 3.1 %while.26 = (s32[]{:T(128)}, f32[4,64,64]{2,1,0:T(8,128)S(1)}, f32[4,4,64,64]{3,2,1,0:T(8,128)}, f32[4,4]{1,0:T(4,128)S(1)}, f32[4,4,64,64]{3,2,1,0:T(8,128)S(1)}, /*index=5*/s32[]{:T(128)}, s32[]{:T(128)}) while((s32[]{:T(128)}, f32[4,64,64]{2,1,0:T(8,128)S(1)}, f32[4,4,64,64]{3,2,1,0:T(8,128)}, f32[4,4]{1,0:T(4,128)S(1)}, ...), condition=%wide.region_3.4_spmd.clone, body=%wide.region_2.3_spmd.clone.sunk | while | flops 65539 | bytes 393872 | solution.py:164
  125.4 35.0 %all-gather = f32[32,64,64]{2,1,0:T(8,128)S(1)} all-gather(f32[4,64,64]{2,1,0:T(8,128)S(1)} %get-tuple-element.78), channel_id=2, replica_groups=mesh['sp'=8,'tp'=4] {'sp'}, dimensions={0}, use_global_device_ids=true | all-gather | bytes 589824 | tf_op jit(solution)/shard_map/all_gather | solution.py:22
  160.6 1.3 fusion.7
  161.9 1.6 fusion.6
  163.5 2.9 %fusion.3 = f32[4,128,128,4]{1,2,3,0:T(8,128)S(1)} fusion(f32[4,128,4]{1,2,0:T(4,128)} %copy.69, pred[128,128]{0,1:T(8,128)(4,1)} %iota_compare_fusion, f32[4,128,64]{1,2,0:T(8,128)S(1)} %get-tuple-element.152, f32[4,128,64]{1,2,0:T(8,128)} %copy-done.2), kind=kOutput, calls=%fused_computation.15 | convolution fusion | flops 202113024 | bytes 1335296 | tf_op jit(solution)/shard_map/blhn,bshn->blsh/dot_general | solution.py:153
  166.5 1.1 fusion.5
  168.2 5.7 %psum.7 = f32[512]{0:T(512)S(1)} all-reduce(f32[512]{0:T(512)S(1)} %get-tuple-element.137), channel_id=1, replica_groups=mesh['sp'=8,'tp'=4] {'tp'}, use_global_device_ids=true, to_apply=%region_8.9 | all-reduce | flops 512 | bytes 4096 | tf_op jit(solution)/shard_map/psum | solution.py:190
  174.0 1.0 maximum_convert_fusion.1
  176.9 4.8 %fusion.23 = f32[512,2048]{1,0:T(8,128)} fusion(bf16[512,2048]{1,0:T(8,128)(2,1)} %all-gather.8.cloned.1.call-done, bf16[512,256]{0,1:T(8,128)(2,1)S(1)} %multiply_convert_fusion.1, bf16[512,256]{0,1:T(8,128)(2,1)S(1)} %fusion.8), kind=kOutput, calls=%fused_computation.53 | convolution fusion | flops 1074790400 | bytes 6815744 | tf_op jit(solution)/shard_map/dot_general | solution.py:196
  181.7 48.6 %reduce-scatter.2.cloned.1.call-done = f32[512,512]{1,0:T(8,128)} async-done(((f32[512,2048]{1,0:T(8,128)}), f32[512,512]{1,0:T(8,128)}) %reduce-scatter.2.cloned.1.call-update) | async-done | bytes 1048592 | tf_op jit(solution)/shard_map/reduce_scatter | solution.py:201
  230.4 2.1 convert_element_type.83
  (115 shorter events, 16.0 us)
Async XLA Ops:
  6.5 169.8 %copy-start = (bf16[1,256,256]{2,1,0:T(8,128)(2,1)S(1)}, bf16[1,256,256]{2,1,0:T(8,128)(2,1)}, u32[]{:S(2)}) copy-start(bf16[1,256,256]{2,1,0:T(8,128)(2,1)} %param.32) | copy-start | bytes 393220
  6.5 4.5 %copy-start.1 = (bf16[512,512]{1,0:T(8,128)(2,1)S(1)}, bf16[512,512]{1,0:T(8,128)(2,1)}, u32[]{:S(2)}) copy-start(bf16[512,512]{1,0:T(8,128)(2,1)} %param.24) | copy-start | bytes 1572868
  6.5 80.2 %all-gather.6.cloned.1.call-start = ((), (), s32[]{:S(2)}) async-start(), calls=%async_computation.2 | async-start | bytes 4718592 | tf_op jit(solution)/shard_map/all_gather | solution.py:77
  12.8 4.4 %copy-start.3 = (bf16[256,256]{1,0:T(8,128)(2,1)S(1)}, bf16[256,256]{1,0:T(8,128)(2,1)}, u32[]{:S(2)}) copy-start(bf16[256,256]{1,0:T(8,128)(2,1)} %param.43) | copy-start | bytes 393220
  12.8 4.4 %copy-start.4 = (bf16[256,256]{1,0:T(8,128)(2,1)S(1)}, bf16[256,256]{1,0:T(8,128)(2,1)}, u32[]{:S(2)}) copy-start(bf16[256,256]{1,0:T(8,128)(2,1)} %param.42) | copy-start | bytes 393220
  12.8 5.3 %copy-start.16 = (bf16[512]{0:T(512)(128)(2,1)S(1)}, bf16[512]{0:T(512)(128)(2,1)}, u32[]{:S(2)}) copy-start(bf16[512]{0:T(512)(128)(2,1)} %param.25) | copy-start | bytes 3076
  12.8 31.1 %copy-start.18 = (f32[4]{0:T(128)S(1)}, f32[4]{0:T(128)}, u32[]{:S(2)}) copy-start(f32[4]{0:T(128)} %param.40) | copy-start | bytes 52
  12.8 32.5 %copy-start.10 = (f32[4,256]{1,0:T(4,128)S(1)}, f32[4,256]{1,0:T(4,128)}, u32[]{:S(2)}) copy-start(f32[4,256]{1,0:T(4,128)} %param.34) | copy-start | bytes 12292
  12.8 32.5 %copy-start.12 = (f32[4,64]{1,0:T(4,128)S(1)}, f32[4,64]{1,0:T(4,128)}, u32[]{:S(2)}) copy-start(f32[4,64]{1,0:T(4,128)} %param.36) | copy-start | bytes 3076
  12.8 32.5 %copy-start.13 = (f32[4,64]{1,0:T(4,128)S(1)}, f32[4,64]{1,0:T(4,128)}, u32[]{:S(2)}) copy-start(f32[4,64]{1,0:T(4,128)} %param.35) | copy-start | bytes 3076
  12.8 33.8 %copy-start.20 = (f32[4]{0:T(128)S(1)}, f32[4]{0:T(128)}, u32[]{:S(2)}) copy-start(f32[4]{0:T(128)} %param.38) | copy-start | bytes 52
  12.8 33.8 %all-to-all-start = ((bf16[4,512,512]{1,2,0:T(8,128)(2,1)}), bf16[4,512,512]{1,2,0:T(8,128)(2,1)S(1)}, u32[]{:S(2)}, u32[]{:S(2)}) async-start(bf16[4,512,512]{1,2,0:T(8,128)(2,1)} %stack.22), calls=%async_computation | async-start | bytes 4194304 | tf_op jit(solution)/shard_map/all_to_all | solution.py:80
  17.2 159.7 %all-gather.8.cloned.1.call-start = ((), (), s32[]{:S(2)}) async-start(), calls=%async_computation.3 | async-start | bytes 2359296 | tf_op jit(solution)/shard_map/all_gather | solution.py:198
  18.0 212.4 %reduce-scatter.2.cloned.1.call-start = ((), (), s32[]{:S(2)}) async-start(), calls=%async_computation.4 | async-start | bytes 5242880 | tf_op jit(solution)/shard_map/reduce_scatter | solution.py:201
  49.0 45.2 %copy-start.9 = (f32[512,4]{0,1:T(4,128)S(1)}, f32[512,4]{0,1:T(4,128)}, u32[]{:S(2)}) copy-start(f32[512,4]{0,1:T(4,128)} %param.39) | copy-start | bytes 24580
  49.0 45.2 %copy-start.17 = (f32[4]{0:T(128)S(1)}, f32[4]{0:T(128)}, u32[]{:S(2)}) copy-start(f32[4]{0:T(128)} %param.37) | copy-start | bytes 52
  91.8 28.1 %collective-permute-start.1 = (bf16[3,384]{0,1:T(8,128)(2,1)S(1)}, bf16[3,384]{0,1:T(8,128)(2,1)S(1)}, u32[]{:S(2)}, u32[]{:S(2)}) collective-permute-start(bf16[3,384]{0,1:T(8,128)(2,1)S(1)} %slice.152), channel_id=1, source_target_pairs={{0,4},{4,8},{8,12},{12,16},{16,20},{20,24},{24,28},{1,5},{5,9},{9,... | collective-permute-start | bytes 6920 | tf_op jit(solution)/shard_map/ppermute | solution.py:17
  95.0 25.1 %copy-start.5 = (f32[384]{0:T(512)S(1)}, f32[384]{0:T(512)}, u32[]{:S(2)}) copy-start(f32[384]{0:T(512)} %get-tuple-element.113) | copy-start | bytes 4612
  95.0 25.1 %copy-start.6 = (f32[384]{0:T(512)S(1)}, f32[384]{0:T(512)}, u32[]{:S(2)}) copy-start(f32[384]{0:T(512)} %get-tuple-element.114) | copy-start | bytes 4612
  95.0 25.1 %copy-start.7 = (f32[384]{0:T(512)S(1)}, f32[384]{0:T(512)}, u32[]{:S(2)}) copy-start(f32[384]{0:T(512)} %get-tuple-element.115) | copy-start | bytes 4612
  95.0 25.1 %copy-start.8 = (f32[384]{0:T(512)S(1)}, f32[384]{0:T(512)}, u32[]{:S(2)}) copy-start(f32[384]{0:T(512)} %get-tuple-element.116) | copy-start | bytes 4612
  98.0 76.0 %collective-permute-start = (bf16[15,256]{0,1:T(8,128)(2,1)}, bf16[15,256]{0,1:T(8,128)(2,1)}, u32[]{:S(2)}, u32[]{:S(2)}) collective-permute-start(bf16[15,256]{0,1:T(8,128)(2,1)} %slice.139), channel_id=1, source_target_pairs={{0,4},{4,8},{8,12},{12,16},{16,20},{20,24},{24,28},{1,5},{5,9},{9,... | collective-permute-start | bytes 23048 | tf_op jit(solution)/shard_map/ppermute | solution.py:17
  166.5 1.5 copy-start.11
  167.6 6.3 %copy-start.15 = (f32[256]{0:T(256)S(1)}, f32[256]{0:T(256)}, u32[]{:S(2)}) copy-start(f32[256]{0:T(256)} %param.41) | copy-start | bytes 3076
  (3 other events, 2.3 us)
Sparse Core Ops, SparseCore 0:
  11.1 75.5 all-gather.5
  88.7 60.9 all-gather.7
  181.9 48.4 reduce-scatter.1
